TPU v7x, 256 devices: a 4x2x16 block of a 4x16x16 slice. The times are simulated.
256 devices in a mesh: grp: 2 (over y), sp: 16 (over z), tp: 8 (over x, core).
Axes of the slice: x: 4, y: 2, z: 16, core: 2. Of those that a mesh axis runs over, the one named last changes fastest.
The devices are a block of a 4x16x16 slice.
Arguments:
- tokens: bfloat16 [2, 16384, 2048], P('grp', ('sp', 'tp')), parts along dimension 0, may hold values from -6 to 6
- norm_gain: bfloat16 [2048], replicated, may hold values from 0.099609375 to 1.8984375
- w_query: bfloat16 [2048, 1024], P('sp'), may hold values from -0.125 to 0.125
- w_forget: bfloat16 [2048, 1024], P('sp'), may hold values from -0.125 to 0.125
- w_input: bfloat16 [2048, 1024], P('sp'), may hold values from -0.125 to 0.125
- floor_gap: float32 [1024], replicated, may hold values from 1.8310547e-05 to 0.12
- extra_decay: float32 [2, 16384, 16], P('grp', ('sp', 'tp')), parts along dimension 0, may hold values from -1.4 to 0, as said below
- init_state: float32 [2, 16, 64, 64], P('grp'), parts along dimension 0, may hold values from -0.03125 to 0.03125
- head_norm_gain: bfloat16 [1024], replicated, may hold values from 0.099609375 to 1.8984375
- w_output: bfloat16 [1024, 2048], P(None, 'sp'), may hold values from -0.1875 to 0.1875
Outputs:
- mixed: bfloat16 [2, 16384, 2048], P('grp', ('sp', 'tp')), parts along dimension 0
- final_state: float32 [2, 65536], P('grp', ('sp', 'tp')), parts along dimension 0
There are 2 independent parts, one for each index of `grp`. A program takes and returns all parts, laid end to end along the dimension named above; an argument that names none is the same for every part. Nothing has to cross between parts.
Inputs may be any that keep to these rules, and one draw needn't show every extreme that they name: `extra_decay`: no entry is positive.
All inputs are finite; a program needn't handle non-finite values.
Results may differ from a plain program's by a relative error of at most 0.014.
Values may be sent and summed in bfloat16 or wider, within the bound.
A program may use at most 128 MiB of HBM per device.

v0:
```python
import jax
import jax.numpy as jnp
from jax import lax
from jax.sharding import Mesh
from jax.sharding import PartitionSpec as P

HEADS = 16
HEAD = 64
BLOCK = 64
SP_TP = ("sp", "tp_0", "tp_1")
EPSILON = 1e-05


def nothing_yet(value, identity):
    return jax.tree.map(
        lambda a, e: jnp.broadcast_to(jnp.asarray(e, a.dtype), a.shape), value, identity
    )


def entering_2(value, axes, combine, identity):
    before = start = nothing_yet(value, identity)
    total = value
    for axis in reversed(axes):
        peers, mine = (lax.axis_size(axis), lax.axis_index(axis))
        pieces = jax.tree.map(
            lambda part, kind: lax.all_gather(part.astype(kind), axis),
            total,
            (jnp.bfloat16, jnp.bfloat16),
        )
        inside, total = (start, start)
        for k in range(peers):
            passed = k < mine
            total = combine(
                total, jax.tree.map(lambda part, own: part[k].astype(own.dtype), pieces, value)
            )
            inside = jax.tree.map(lambda new, old: jnp.where(passed, new, old), total, inside)
        before = combine(inside, before)
    return before


def prefix_by_axis(value, axes, combine, identity):
    before = start = nothing_yet(value, identity)
    total = value
    for axis in reversed(axes):
        peers, mine = (lax.axis_size(axis), lax.axis_index(axis))
        pieces = lax.all_gather(total, axis)
        inside, total = (start, start)
        for k in reversed(range(peers)):
            passed = k > mine
            total = combine(total, pieces[k])
            inside = jnp.where(passed, total, inside)
        before = combine(inside, before)
    return before


def reduced_to_own(pieces, axes, order):
    inside = pieces.shape[1:]
    pieces = pieces.reshape(*(lax.axis_size(a) for a in axes), *inside)
    pieces = jnp.moveaxis(pieces, order, range(len(axes))).reshape(-1, *inside)
    for k in order:
        pieces = lax.psum_scatter(pieces, axes[k], scatter_dimension=0, tiled=True)
    return pieces[0]


def in_blocks(value, dim, peers):
    lengths = value.shape
    pieces = value.reshape(*lengths[:dim], peers, lengths[dim] // peers, *lengths[dim + 1 :])
    return jnp.moveaxis(pieces, dim, 0)


def summed_rows(value, axes, order, dim):
    peers = lax.axis_size(axes)
    return reduced_to_own(in_blocks(value, dim, peers), axes, order)


def layer_normed(tokens, norm_gain):
    values = tokens.astype(jnp.float32)
    center = values - jnp.mean(values, axis=-1, keepdims=True)
    spread = jnp.mean(center * center, axis=-1, keepdims=True)
    return (center * lax.rsqrt(spread + EPSILON) * norm_gain.astype(jnp.float32)).astype(
        jnp.bfloat16
    )


def gate_terms(query_sum, forget_sum, input_sum, floor_gap, extra_decay):
    query_raw = query_sum.astype(jnp.bfloat16)
    forget_raw = forget_sum.astype(jnp.bfloat16)
    input_raw = input_sum.astype(jnp.bfloat16)
    forget_pre = forget_raw.astype(jnp.float32)
    split_shape = forget_pre.shape[:-1] + (HEADS, HEAD)
    log_keep = jnp.logaddexp(
        jnp.log1p(-floor_gap), jnp.log(floor_gap) + jax.nn.log_sigmoid(forget_pre)
    )
    log_keep = log_keep.reshape(split_shape) + extra_decay[..., None]
    key_gate = (floor_gap * jax.nn.sigmoid(-forget_pre)).reshape(split_shape)
    query = jax.nn.silu(query_raw.astype(jnp.float32)).reshape(split_shape)
    values = input_raw.astype(jnp.float32).reshape(split_shape)
    return (query, key_gate, values, log_keep)


def block_pass(query, key_gate, values, log_keep):
    highest = lax.Precision.HIGHEST
    cumul = jnp.cumsum(log_keep, axis=2)
    q_decayed = query * jnp.exp(cumul)
    key_decayed = key_gate * jnp.exp(-cumul)
    causal = lax.broadcasted_iota(jnp.int32, (BLOCK, BLOCK), 0) >= lax.broadcasted_iota(
        jnp.int32, (BLOCK, BLOCK), 1
    )
    scores = jnp.einsum("snthd,snuhd->snhtu", q_decayed, key_decayed, precision=highest)
    scores = jnp.where(causal, scores, 0.0)
    within = jnp.einsum("snhtu,snuhe->snthe", scores, values, precision=highest)
    totals = cumul[:, :, -1]
    k_tail = key_gate * jnp.exp(totals[:, :, None] - cumul)
    block_state = jnp.einsum("snthd,snthe->snhde", k_tail, values, precision=highest)
    return (q_decayed, within, totals, block_state)


def linked_advance(earlier, later):
    return (earlier[0] + later[0], jnp.exp(later[0])[..., None] * earlier[1] + later[1])


def add_logs(earlier, later):
    return earlier + later


def read_out(q_global, leading_logarithm, prefix_state, init_part):
    carried = jnp.exp(leading_logarithm)[..., None] * init_part + prefix_state
    added = jnp.einsum("snthd,shde->snthe", q_global, carried, precision=lax.Precision.HIGHEST)
    return (carried, added)


def body(
    tokens,
    norm_gain,
    w_query,
    w_forget,
    w_input,
    floor_gap,
    extra_decay,
    init_state,
    head_norm_gain,
    w_output,
):
    normed = layer_normed(tokens, norm_gain)
    seqs, span = (tokens.shape[0], tokens.shape[1])

    def add_rows(piece):
        return jnp.dot(normed, piece, preferred_element_type=jnp.float32)

    query_sum = add_rows(lax.all_gather(w_query, "sp", axis=0, tiled=True))
    forget_sum = add_rows(lax.all_gather(w_forget, "sp", axis=0, tiled=True))
    input_sum = add_rows(lax.all_gather(w_input, "sp", axis=0, tiled=True))
    query, key_gate, values, log_keep = gate_terms(
        query_sum, forget_sum, input_sum, floor_gap, extra_decay
    )
    blocks = span // BLOCK
    blocked = (seqs, blocks, BLOCK, HEADS, HEAD)
    q_decayed, within, totals, block_state = block_pass(
        query.reshape(blocked),
        key_gate.reshape(blocked),
        values.reshape(blocked),
        log_keep.reshape(blocked),
    )
    running_state = jnp.zeros((seqs, HEADS, HEAD, HEAD), jnp.float32)
    running_log = jnp.zeros((seqs, HEADS, HEAD), jnp.float32)
    entering_list = []
    offset_list = []
    for number in range(blocks):
        entering_list.append(running_state)
        offset_list.append(running_log)
        running_state = (
            jnp.exp(totals[:, number])[..., None] * running_state + block_state[:, number]
        )
        running_log = running_log + totals[:, number]
    entering = jnp.stack(entering_list, axis=1)
    offsets = jnp.stack(offset_list, axis=1)
    local_out = within + jnp.einsum(
        "snthd,snhde->snthe", q_decayed, entering, precision=lax.Precision.HIGHEST
    )
    q_global = q_decayed * jnp.exp(offsets[:, :, None])
    leading_logarithm, prefix_state = entering_2(
        (running_log, running_state),
        SP_TP,
        linked_advance,
        (jnp.zeros_like(running_log), jnp.zeros_like(running_state)),
    )
    carried, added = read_out(q_global, leading_logarithm, prefix_state, init_state)
    flat_total = HEADS * HEAD * HEAD
    piece_count = flat_total // lax.axis_size(SP_TP)
    piece_start = lax.axis_index(SP_TP) * piece_count
    later_log = prefix_by_axis(running_log, SP_TP, add_logs, jnp.zeros_like(running_log))
    surviving = (jnp.exp(later_log)[..., None] * running_state).reshape(seqs, flat_total)
    summed = summed_rows(surviving.astype(jnp.bfloat16), SP_TP, (2, 0, 1), 1).astype(jnp.float32)
    initial_part = (
        jnp.exp(leading_logarithm + running_log + later_log)[..., None] * init_state
    ).reshape(seqs, flat_total)
    final_state = lax.dynamic_slice_in_dim(initial_part, piece_start, piece_count, 1) + summed
    recurrent = (local_out + added).reshape(seqs, span, HEADS, HEAD)
    average_power = jnp.mean(recurrent * recurrent, axis=-1, keepdims=True)
    scaled = (
        recurrent
        * lax.rsqrt(average_power + EPSILON)
        * head_norm_gain.astype(jnp.float32).reshape(HEADS, HEAD)
    )
    gated = scaled.reshape(seqs, span, HEADS * HEAD).astype(jnp.bfloat16)
    mixed = jnp.dot(
        gated,
        lax.all_gather(w_output, "sp", axis=1, tiled=True),
        preferred_element_type=jnp.float32,
    ).astype(jnp.bfloat16)
    return (mixed, final_state)


def solution(mesh):
    torus = Mesh(
        mesh.devices.reshape(mesh.shape["grp"], mesh.shape["sp"], 4, 2),
        ("grp", "sp", "tp_0", "tp_1"),
    )
    in_specs = (
        P("grp", SP_TP, None),
        P(),
        P("sp", None),
        P("sp", None),
        P("sp", None),
        P(),
        P("grp", SP_TP, None),
        P("grp", None, None, None),
        P(),
        P(None, "sp"),
    )
    out_specs = (P("grp", SP_TP, None), P("grp", SP_TP))
    return jax.shard_map(body, mesh=torus, in_specs=in_specs, out_specs=out_specs, check_vma=False)
```

profile of v0, /device:TPU:36, one launch (start us, length us, event | category | flops | bytes accessed | tf_op | source)
XLA Modules:
  0.0 588.2 jit_solution(18242492222280507001)
XLA Ops:
  12.4 1.3 fusion.7
  14.5 85.1 %all-gather.10.cloned.1.call-done = bf16[2048,1024]{1,0:T(8,128)(2,1)} async-done(((bf16[128,1024]{1,0:T(8,128)(2,1)}), bf16[2048,1024]{1,0:T(8,128)(2,1)}) %all-gather.10.cloned.1.call-update) | async-done | bytes 4194320 | tf_op jit(solution)/shard_map/all_gather | solution.py:151
  99.6 3.8 add_select_fusion
  104.2 1.9 all_gather.51
  106.1 1.9 all_gather.58
  108.5 10.8 %all_gather.52 = bf16[4,1,16,64]{3,2,1,0:T(8,128)(2,1)S(1)} all-gather(bf16[1,1,16,64]{3,2,1,0:T(8,128)(2,1)S(1)} %get-tuple-element.47), channel_id=1, replica_groups=mesh['grp'=2,'sp'=16,'tp_0'=4,'tp_1'=2] {'tp_0'}, dimensions={0}, use_global_device_ids=true | all-gather | bytes 10240 | tf_op jit(solution)/shard_map/all_gather | solution.py:26
  119.4 11.9 %all_gather.59 = f32[4,1,16,64]{3,2,1,0:T(8,128)S(1)} all-gather(f32[1,1,16,64]{3,2,1,0:T(8,128)S(1)} %slice_add_fusion.18), channel_id=1, replica_groups=mesh['grp'=2,'sp'=16,'tp_0'=4,'tp_1'=2] {'tp_0'}, dimensions={0}, use_global_device_ids=true | all-gather | bytes 20480 | tf_op jit(solution)/shard_map/all_gather | solution.py:46
  131.3 29.1 %all_gather.53 = bf16[16,1,16,64]{3,2,1,0:T(8,128)(2,1)S(1)} all-gather(bf16[1,1,16,64]{3,2,1,0:T(8,128)(2,1)S(1)} %get-tuple-element.37), channel_id=1, replica_groups=mesh['grp'=2,'sp'=16,'tp_0'=4,'tp_1'=2] {'sp'}, dimensions={0}, use_global_device_ids=true | all-gather | bytes 34816 | tf_op jit(solution)/shard_map/all_gather | solution.py:26
  160.4 26.9 %all_gather.60 = f32[16,1,16,64]{3,2,1,0:T(8,128)S(1)} all-gather(f32[1,1,16,64]{3,2,1,0:T(8,128)S(1)} %slice_add_fusion.15), channel_id=1, replica_groups=mesh['grp'=2,'sp'=16,'tp_0'=4,'tp_1'=2] {'sp'}, dimensions={0}, use_global_device_ids=true | all-gather | bytes 69632 | tf_op jit(solution)/shard_map/all_gather | solution.py:46
  188.4 1.3 reshape_reshape.8
  189.7 3.1 divide_multiply_fusion.1
  192.8 1.2 reshape_reshape.7
  194.0 55.5 %all-gather.6.cloned.1.call-done = bf16[2048,1024]{1,0:T(8,128)(2,1)} async-done(((bf16[128,1024]{1,0:T(8,128)(2,1)}), bf16[2048,1024]{1,0:T(8,128)(2,1)}) %all-gather.6.cloned.1.call-update) | async-done | bytes 4194320 | tf_op jit(solution)/shard_map/all_gather | solution.py:152
  249.5 3.0 convolution_convert_fusion.3
  252.8 3.3 fusion.16
  257.3 1.2 add_convert_fusion
  261.2 1.5 fusion.154
  263.6 2.6 all_gather.54
  266.6 14.0 %all_gather.55 = bf16[4,1,16,64,64]{4,3,2,1,0:T(8,128)(2,1)} all-gather(bf16[1,1,16,64,64]{4,3,2,1,0:T(8,128)(2,1)S(1)} %fusion.36), channel_id=1, replica_groups=mesh['grp'=2,'sp'=16,'tp_0'=4,'tp_1'=2] {'tp_0'}, dimensions={0}, use_global_device_ids=true | all-gather | bytes 655360 | tf_op jit(solution)/shard_map/all_gather | solution.py:26
  280.7 2.5 fusion.52
  284.0 1.3 dynamic-slice
  287.2 2.0 broadcast_multiply_fusion.1
  289.2 1.4 reshape.2016
  291.8 2.4 convolution_select_fusion
  295.3 3.0 fusion.1
  298.3 114.6 %all-reduce.6.cloned.1.call-done = bf16[64,1,512]{2,0,1:T(8,128)(2,1)} async-done(((bf16[64,1,512]{2,0,1:T(8,128)(2,1)}), bf16[64,1,512]{2,0,1:T(8,128)(2,1)}) %all-reduce.6.cloned.1.call-update) | async-done | bytes 65552
  413.6 8.3 %all-reduce.3 = bf16[4,1,512]{2,0,1:T(4,128)(2,1)S(1)} all-reduce(bf16[4,1,512]{2,0,1:T(4,128)(2,1)S(1)} %constant_dynamic-slice_fusion), channel_id=4, replica_groups=mesh['grp'=2,'sp'=16,'tp_0'=4,'tp_1'=2] {'tp_0'}, use_global_device_ids=true, to_apply=%region_6.7.clone | all-reduce | flops 2048 | bytes 8192
  423.1 63.5 %all-gather.12.cloned.1.call-done = bf16[16,1,16,64,64]{4,3,2,1,0:T(8,128)(2,1)} async-done(((bf16[1,1,16,64,64]{4,3,2,1,0:T(8,128)(2,1)}), bf16[16,1,16,64,64]{4,3,2,1,0:T(8,128)(2,1)}) %all-gather.12.cloned.1.call-update) | async-done | bytes 2097168 | tf_op jit(solution)/shard_map/all_gather | solution.py:26
  486.6 10.3 %multiply_reduce_fusion = (f32[2,64,16]{1,2,0:T(8,128)S(1)}, f32[1,2,64,16,64]{2,4,3,1,0:T(8,128)}) fusion(f32[1,2,64,16,64]{2,4,3,1,0:T(8,128)} %fusion.1, f32[2,64,16,64]{3,2,1,0:T(8,128)S(1)} %copy-done.3, f32[1,16,64,64]{3,2,1,0:T(8,128)} %param.17, bf16[16,1,16,64,64]{4,3,2,1,0:T(8,128)(2,1)} %all-gather.12.cloned.1.call-done, ...), kind=kOutput, calls=%fused_computation.33 | convolution fusion | flops 107018240 | bytes 4829206 | tf_op jit(solution)/shard_map/snthd,shde->snthe/dot_general | solution.py:128
  497.0 1.7 copy.73
  499.4 78.2 %all-gather.14.cloned.1.call-done = bf16[1024,2048]{1,0:T(8,128)(2,1)} async-done(((bf16[1024,128]{1,0:T(8,128)(2,1)}), bf16[1024,2048]{1,0:T(8,128)(2,1)}) %all-gather.14.cloned.1.call-update) | async-done | bytes 4194320 | tf_op jit(solution)/shard_map/all_gather | solution.py:208
  577.6 3.7 fusion
  (96 shorter events, 20.7 us)
Async XLA Ops:
  7.2 92.5 %all-gather.10.cloned.1.call-start = ((), (), s32[]{:S(2)}) async-start(), calls=%async_computation.3 | async-start | bytes 4456448 | tf_op jit(solution)/shard_map/all_gather | solution.py:151
  8.0 181.7 %all-gather.8.cloned.1.call-start = ((), (), s32[]{:S(2)}) async-start(), calls=%async_computation.2 | async-start | bytes 4456448 | tf_op jit(solution)/shard_map/all_gather | solution.py:150
  8.8 240.7 %all-gather.6.cloned.1.call-start = ((), (), s32[]{:S(2)}) async-start(), calls=%async_computation.1 | async-start | bytes 4456448 | tf_op jit(solution)/shard_map/all_gather | solution.py:152
  9.6 271.0 %reduce-scatter.4.cloned.1.call-start = ((), (), s32[]{:S(2)}) async-start(), calls=%async_computation.6 | async-start | bytes 196608 | tf_op jit(solution)/shard_map/reduce_scatter | solution.py:61
  10.4 93.0 %copy-start.9 = (f32[2048]{0:T(1024)}, f32[2048]{0:T(1024)S(1)}, u32[]{:S(2)}) copy-start(f32[2048]{0:T(1024)S(1)} %convert_element_type.904) | copy-start | bytes 24580
  12.4 91.0 %copy-start.12 = (f32[128]{0:T(128)}, f32[128]{0:T(128)S(1)}, u32[]{:S(2)}) copy-start(f32[128]{0:T(128)S(1)} %broadcast_multiply_fusion.2) | copy-start | bytes 1540
  13.8 89.7 %copy-start.15 = (f32[128]{0:T(128)}, f32[128]{0:T(128)S(1)}, u32[]{:S(2)}) copy-start(f32[128]{0:T(128)S(1)} %add_rsqrt_fusion.1) | copy-start | bytes 1540
  103.4 86.3 %copy-start.1 = (bf16[1,128,2048]{2,1,0:T(8,128)(2,1)S(1)}, bf16[1,128,2048]{2,1,0:T(8,128)(2,1)}, u32[]{:S(2)}) copy-start(bf16[1,128,2048]{2,1,0:T(8,128)(2,1)} %param.10) | copy-start | bytes 1572868
  189.7 59.8 %copy-start.10 = (f32[2048]{0:T(1024)S(1)}, f32[2048]{0:T(1024)}, u32[]{:S(2)}) copy-start(f32[2048]{0:T(1024)} %copy-done.9) | copy-start | bytes 24580
  189.7 59.8 %copy-start.13 = (f32[128]{0:T(128)S(1)}, f32[128]{0:T(128)}, u32[]{:S(2)}) copy-start(f32[128]{0:T(128)} %copy-done.12) | copy-start | bytes 1540
  189.7 59.8 %copy-start.16 = (f32[128]{0:T(128)S(1)}, f32[128]{0:T(128)}, u32[]{:S(2)}) copy-start(f32[128]{0:T(128)} %copy-done.15) | copy-start | bytes 1540
  260.0 27.1 %copy-start.4 = (f32[16,64]{1,0:T(8,128)S(1)}, f32[16,64]{1,0:T(8,128)}, u32[]{:S(2)}) copy-start(f32[16,64]{1,0:T(8,128)} %get-tuple-element.2) | copy-start | bytes 12292
  260.2 25.1 %copy-start.14 = (u32[256]{0:T(256)S(1)}, u32[256]{0:T(256)}, u32[]{:S(2)}) copy-start(u32[256]{0:T(256)} %constant.88) | copy-start | bytes 3076
  260.2 25.7 %copy-start.11 = (bf16[1024]{0:T(1024)(128)(2,1)S(1)}, bf16[1024]{0:T(1024)(128)(2,1)}, u32[]{:S(2)}) copy-start(bf16[1024]{0:T(1024)(128)(2,1)} %param.18) | copy-start | bytes 6148
  261.2 29.4 %copy-start.6 = (f32[16,64]{1,0:T(8,128)S(1)}, f32[16,64]{1,0:T(8,128)}, u32[]{:S(2)}) copy-start(f32[16,64]{1,0:T(8,128)} %get-tuple-element.4) | copy-start | bytes 12292
  261.2 30.0 %copy-start.5 = (f32[16,64]{1,0:T(8,128)S(1)}, f32[16,64]{1,0:T(8,128)}, u32[]{:S(2)}) copy-start(f32[16,64]{1,0:T(8,128)} %get-tuple-element.5) | copy-start | bytes 12292
  261.2 30.6 %copy-start = (f32[2,64,16,64]{3,2,1,0:T(8,128)S(1)}, f32[2,64,16,64]{3,2,1,0:T(8,128)}, u32[]{:S(2)}) copy-start(f32[2,64,16,64]{3,2,1,0:T(8,128)} %get-tuple-element.13) | copy-start | bytes 1572868
  263.5 149.4 %all-reduce.6.cloned.1.call-start = ((), (), s32[]{:S(2)}) async-start(), calls=%async_computation.7 | async-start | bytes 131072
  280.6 206.0 %all-gather.12.cloned.1.call-start = ((), (), s32[]{:S(2)}) async-start(), calls=%async_computation.4 | async-start | bytes 4456448 | tf_op jit(solution)/shard_map/all_gather | solution.py:26
  283.2 294.4 %all-gather.14.cloned.1.call-start = ((), (), s32[]{:S(2)}) async-start(), calls=%async_computation.5 | async-start | bytes 4456448 | tf_op jit(solution)/shard_map/all_gather | solution.py:208
  290.6 4.7 copy-start.2
  291.8 194.8 %copy-start.8 = (f32[16,64]{1,0:T(8,128)S(1)}, f32[16,64]{1,0:T(8,128)}, u32[]{:S(2)}) copy-start(f32[16,64]{1,0:T(8,128)} %get-tuple-element.45) | copy-start | bytes 12292
  294.2 192.4 %copy-start.3 = (f32[2,64,16,64]{3,2,1,0:T(8,128)S(1)}, f32[2,64,16,64]{3,2,1,0:T(8,128)}, u32[]{:S(2)}) copy-start(f32[2,64,16,64]{3,2,1,0:T(8,128)} %get-tuple-element.16) | copy-start | bytes 1572868
  496.9 80.7 %copy-start.7 = (f32[1024]{0:T(1024)S(1)}, f32[1024]{0:T(1024)}, u32[]{:S(2)}) copy-start(f32[1024]{0:T(1024)} %convert_element_type.1001) | copy-start | bytes 12292
Sparse Core Ops, SparseCore 0:
  9.8 89.7 all-gather.9
  101.4 73.5 all-gather.7
  176.8 72.5 all-gather.5
  263.6 13.2 reduce-scatter.3
  280.7 132.1 all-reduce.5
  414.6 72.0 all-gather.11
  488.4 89.1 all-gather.13
where the time goes:
time: 589 us; the launch traced here: 588 us
  waiting for transfers between devices  400 us (68%)
  blocking collectives  107 us (18%)
  matrix products  31.4 us (5%)
  other arithmetic  18.4 us (3%)
  local copies, waits for them, and re-layouts  15.3 us (3%)
  between operations  15.2 us (3%)
    unnamed x8, waiting for transfers between devices  118 us
    all_gather x1, waiting for transfers between devices, body(): forget_sum = add_rows(lax.all_gather(w_forget, 'sp', axis=0, tiled=True))  85.1 us
    all_gather x1, waiting for transfers between devices, body(): lax.all_gather(w_output, 'sp', axis=1, tiled=True)  78.2 us
    all_gather x1, waiting for transfers between devices, entering_2(): lax.all_gather(part.astype(kind), axis)  63.5 us
    all_gather x5, blocking collectives, entering_2(): lax.all_gather(part.astype(kind), axis)  58.3 us
    all_gather x1, waiting for transfers between devices, body(): input_sum = add_rows(lax.all_gather(w_input, 'sp', axis=0, tiled=True))  55.5 us
    all_gather x3, blocking collectives, prefix_by_axis(): pieces = lax.all_gather(total, axis)  40.7 us
  transfers between devices with their start and end apart: 7, of which 5 were waited for; matrix products, arithmetic and copies ran while one was open for 8% of the time, Pallas kernels for 0%

commit v1 on v0

--- a/solution.py
+++ b/solution.py
@@ -9,6 +9,19 @@
 BLOCK = 64
 SP_TP = ("sp", "tp_0", "tp_1")
 EPSILON = 1e-05
+
+
+def ring_gather(x, axis, dim):
+    ways = lax.axis_size(axis)
+    up = [(d, (d + 1) % ways) for d in range(ways)]
+    down = [(d, (d - 1) % ways) for d in range(ways)]
+    earlier, later = ([x], [x])
+    for _ in range(ways // 2):
+        earlier.append(lax.ppermute(earlier[-1], axis, up))
+    for _ in range((ways - 1) // 2):
+        later.append(lax.ppermute(later[-1], axis, down))
+    line = jnp.concatenate([*earlier[::-1], *later[1:]], axis=dim)
+    return jnp.roll(line, (lax.axis_index(axis) - ways // 2) * x.shape[dim], axis=dim)
 
 
 def nothing_yet(value, identity):
@@ -204,9 +217,7 @@
     )
     gated = scaled.reshape(seqs, span, HEADS * HEAD).astype(jnp.bfloat16)
     mixed = jnp.dot(
-        gated,
-        lax.all_gather(w_output, "sp", axis=1, tiled=True),
-        preferred_element_type=jnp.float32,
+        gated, ring_gather(w_output, "sp", 1), preferred_element_type=jnp.float32
     ).astype(jnp.bfloat16)
     return (mixed, final_state)
 

time: 589 us -> 614 us (1.042)
  waiting for transfers between devices: 400 us -> 349 us
  local copies, waits for them, and re-layouts: 15.3 us -> 64.4 us
  starting transfers between devices: 0.44 us -> 26.3 us
    ppermute x0 -> x15, waiting for transfers between devices: none -> 86.4 us  [the longest x8 86.4 us: ring_gather(): earlier.append(lax.ppermute(earlier[-1], axis, up))]
    all_gather x1, waiting for transfers between devices: 85.1 us -> 0.01 us  [body(): forget_sum = add_rows(lax.all_gather(w_forget, 'sp', axis=0, tiled=True))]
    all_gather x1 -> x0, waiting for transfers between devices: 78.2 us -> none  [body(): lax.all_gather(w_output, 'sp', axis=1, tiled=True)]
    unnamed x37 -> x76, local copies, waits for them, and re-layouts: 2.66 us -> 45.1 us
    all_gather x1, waiting for transfers between devices: 0.01 us -> 36.7 us  [body(): query_sum = add_rows(lax.all_gather(w_query, 'sp', axis=0, tiled=True))]
    ppermute x0 -> x15, starting transfers between devices: none -> 25.7 us  [the longest x7 22.8 us: ring_gather(): later.append(lax.ppermute(later[-1], axis, down))]
    unnamed x8 -> x7, waiting for transfers between devices: 118 us -> 93.1 us
    all_gather x1, waiting for transfers between devices: 55.5 us -> 69.6 us  [body(): input_sum = add_rows(lax.all_gather(w_input, 'sp', axis=0, tiled=True))]
  transfers between devices with their start and end apart: 7 -> 21, of which waited for: 5 -> 11; matrix products, arithmetic and copies ran while one was open for 8% -> 16% of each run, Pallas kernels for 0% -> 0%
where the time goes in v1:
time: 614 us; the launch traced here: 613 us
  waiting for transfers between devices  349 us (57%)
  blocking collectives  107 us (17%)
  local copies, waits for them, and re-layouts  64.4 us (10%)
  matrix products  31.7 us (5%)
  starting transfers between devices  26.3 us (4%)
  other arithmetic  18.3 us (3%)
  between operations  15.4 us (3%)
    unnamed x7, waiting for transfers between devices  93.1 us
    ppermute x8, waiting for transfers between devices, ring_gather(): earlier.append(lax.ppermute(earlier[-1], axis, up))  86.4 us
    all_gather x1, waiting for transfers between devices, body(): input_sum = add_rows(lax.all_gather(w_input, 'sp', axis=0, tiled=True))  69.6 us
    all_gather x1, waiting for transfers between devices, entering_2(): lax.all_gather(part.astype(kind), axis)  63.6 us
    all_gather x5, blocking collectives, entering_2(): lax.all_gather(part.astype(kind), axis)  58.5 us
    unnamed x76, local copies, waits for them, and re-layouts  45.1 us
    all_gather x3, blocking collectives, prefix_by_axis(): pieces = lax.all_gather(total, axis)  40.5 us
    all_gather x1, waiting for transfers between devices, body(): query_sum = add_rows(lax.all_gather(w_query, 'sp', axis=0, tiled=True))  36.7 us
  transfers between devices with their start and end apart: 21, of which 11 were waited for; matrix products, arithmetic and copies ran while one was open for 16% of the time, Pallas kernels for 0%

profile of v1, /device:TPU:36, one launch (start us, length us, event | category | flops | bytes accessed | tf_op | source)
XLA Modules:
  0.0 612.8 jit_solution(17428901384207720806)
XLA Ops:
  9.7 2.9 collective-permute-start
  12.6 26.2 %collective-permute-done = bf16[1024,128]{1,0:T(8,128)(2,1)S(1)} collective-permute-done((bf16[1024,128]{1,0:T(8,128)(2,1)}, bf16[1024,128]{1,0:T(8,128)(2,1)S(1)}, u32[]{:S(2)}, u32[]{:S(2)}) %collective-permute-start) | collective-permute-done | bytes 262176 | tf_op jit(solution)/shard_map/ppermute | solution.py:20
  38.8 3.2 collective-permute-start.8
  42.0 11.9 %collective-permute-done.1 = bf16[1024,128]{1,0:T(8,128)(2,1)S(1)} collective-permute-done((bf16[1024,128]{1,0:T(8,128)(2,1)S(1)}, bf16[1024,128]{1,0:T(8,128)(2,1)S(1)}, u32[]{:S(2)}, u32[]{:S(2)}) %collective-permute-start.1) | collective-permute-done | bytes 262176 | tf_op jit(solution)/shard_map/ppermute | solution.py:20
  53.9 3.2 collective-permute-start.9
  57.2 11.7 %collective-permute-done.2 = bf16[1024,128]{1,0:T(8,128)(2,1)S(1)} collective-permute-done((bf16[1024,128]{1,0:T(8,128)(2,1)S(1)}, bf16[1024,128]{1,0:T(8,128)(2,1)S(1)}, u32[]{:S(2)}, u32[]{:S(2)}) %collective-permute-start.2) | collective-permute-done | bytes 262176 | tf_op jit(solution)/shard_map/ppermute | solution.py:20
  68.9 3.2 collective-permute-start.10
  72.1 11.3 %collective-permute-done.3 = bf16[1024,128]{1,0:T(8,128)(2,1)S(1)} collective-permute-done((bf16[1024,128]{1,0:T(8,128)(2,1)S(1)}, bf16[1024,128]{1,0:T(8,128)(2,1)S(1)}, u32[]{:S(2)}, u32[]{:S(2)}) %collective-permute-start.3) | collective-permute-done | bytes 262176 | tf_op jit(solution)/shard_map/ppermute | solution.py:20
  83.5 3.2 collective-permute-start.11
  86.7 11.4 %collective-permute-done.4 = bf16[1024,128]{1,0:T(8,128)(2,1)S(1)} collective-permute-done((bf16[1024,128]{1,0:T(8,128)(2,1)S(1)}, bf16[1024,128]{1,0:T(8,128)(2,1)S(1)}, u32[]{:S(2)}, u32[]{:S(2)}) %collective-permute-start.4) | collective-permute-done | bytes 262176 | tf_op jit(solution)/shard_map/ppermute | solution.py:20
  99.5 3.2 collective-permute-start.12
  102.7 9.7 %collective-permute-done.5 = bf16[1024,128]{1,0:T(8,128)(2,1)S(1)} collective-permute-done((bf16[1024,128]{1,0:T(8,128)(2,1)S(1)}, bf16[1024,128]{1,0:T(8,128)(2,1)S(1)}, u32[]{:S(2)}, u32[]{:S(2)}) %collective-permute-start.5) | collective-permute-done | bytes 262176 | tf_op jit(solution)/shard_map/ppermute | solution.py:20
  113.9 3.3 collective-permute-start.13
  117.1 4.1 collective-permute-done.6
  128.1 3.4 collective-permute-start.14
  144.2 4.6 add_select_fusion
  152.5 36.7 %all-gather.7.cloned.1.call-done = bf16[2048,1024]{1,0:T(8,128)(2,1)} async-done(((bf16[128,1024]{1,0:T(8,128)(2,1)}), bf16[2048,1024]{1,0:T(8,128)(2,1)}) %all-gather.7.cloned.1.call-update) | async-done | bytes 4194320 | tf_op jit(solution)/shard_map/all_gather | solution.py:163
  189.2 3.0 divide_multiply_fusion.1
  194.0 69.6 %all-gather.5.cloned.1.call-done = bf16[2048,1024]{1,0:T(8,128)(2,1)} async-done(((bf16[128,1024]{1,0:T(8,128)(2,1)}), bf16[2048,1024]{1,0:T(8,128)(2,1)}) %all-gather.5.cloned.1.call-update) | async-done | bytes 4194320 | tf_op jit(solution)/shard_map/all_gather | solution.py:165
  263.6 2.9 convolution_convert_fusion.2
  269.3 10.8 %all_gather.49 = bf16[4,1,16,64]{3,2,1,0:T(8,128)(2,1)S(1)} all-gather(bf16[1,1,16,64]{3,2,1,0:T(8,128)(2,1)S(1)} %get-tuple-element.47), channel_id=1, replica_groups=mesh['grp'=2,'sp'=16,'tp_0'=4,'tp_1'=2] {'tp_0'}, dimensions={0}, use_global_device_ids=true | all-gather | bytes 10240 | tf_op jit(solution)/shard_map/all_gather | solution.py:39
  280.2 3.3 fusion.23
  288.1 29.0 %all_gather.50 = bf16[16,1,16,64]{3,2,1,0:T(8,128)(2,1)S(1)} all-gather(bf16[1,1,16,64]{3,2,1,0:T(8,128)(2,1)S(1)} %get-tuple-element.37), channel_id=1, replica_groups=mesh['grp'=2,'sp'=16,'tp_0'=4,'tp_1'=2] {'sp'}, dimensions={0}, use_global_device_ids=true | all-gather | bytes 34816 | tf_op jit(solution)/shard_map/all_gather | solution.py:39
  318.9 12.0 %all_gather.55 = f32[4,1,16,64]{3,2,1,0:T(8,128)S(1)} all-gather(f32[1,1,16,64]{3,2,1,0:T(8,128)S(1)} %slice_add_fusion.18), channel_id=1, replica_groups=mesh['grp'=2,'sp'=16,'tp_0'=4,'tp_1'=2] {'tp_0'}, dimensions={0}, use_global_device_ids=true | all-gather | bytes 20480 | tf_op jit(solution)/shard_map/all_gather | solution.py:59
  330.9 26.7 %all_gather.56 = f32[16,1,16,64]{3,2,1,0:T(8,128)S(1)} all-gather(f32[1,1,16,64]{3,2,1,0:T(8,128)S(1)} %slice_add_fusion.15), channel_id=1, replica_groups=mesh['grp'=2,'sp'=16,'tp_0'=4,'tp_1'=2] {'sp'}, dimensions={0}, use_global_device_ids=true | all-gather | bytes 69632 | tf_op jit(solution)/shard_map/all_gather | solution.py:59
  368.4 14.6 %all_gather.52 = bf16[4,1,16,64,64]{4,3,2,1,0:T(8,128)(2,1)} all-gather(bf16[1,1,16,64,64]{4,3,2,1,0:T(8,128)(2,1)S(1)} %fusion.43), channel_id=1, replica_groups=mesh['grp'=2,'sp'=16,'tp_0'=4,'tp_1'=2] {'tp_0'}, dimensions={0}, use_global_device_ids=true | all-gather | bytes 655360 | tf_op jit(solution)/shard_map/all_gather | solution.py:39
  423.5 3.1 fusion.8
  426.7 90.8 %all-reduce.6.cloned.1.call-done = bf16[64,1,512]{2,0,1:T(8,128)(2,1)} async-done(((bf16[64,1,512]{2,0,1:T(8,128)(2,1)}), bf16[64,1,512]{2,0,1:T(8,128)(2,1)}) %all-reduce.6.cloned.1.call-update) | async-done | bytes 65552
  518.1 8.3 %all-reduce.3 = bf16[4,1,512]{2,0,1:T(4,128)(2,1)S(1)} all-reduce(bf16[4,1,512]{2,0,1:T(4,128)(2,1)S(1)} %constant_dynamic-slice_fusion), channel_id=4, replica_groups=mesh['grp'=2,'sp'=16,'tp_0'=4,'tp_1'=2] {'tp_0'}, use_global_device_ids=true, to_apply=%region_6.7.clone | all-reduce | flops 2048 | bytes 8192
  527.7 63.6 %all-gather.11.cloned.1.call-done = bf16[16,1,16,64,64]{4,3,2,1,0:T(8,128)(2,1)} async-done(((bf16[1,1,16,64,64]{4,3,2,1,0:T(8,128)(2,1)}), bf16[16,1,16,64,64]{4,3,2,1,0:T(8,128)(2,1)}) %all-gather.11.cloned.1.call-update) | async-done | bytes 2097168 | tf_op jit(solution)/shard_map/all_gather | solution.py:39
  591.3 9.7 %multiply_reduce_fusion = (f32[2,64,16]{1,2,0:T(8,128)S(1)}, f32[1,2,64,16,64]{2,4,3,1,0:T(8,128)S(1)}) fusion(f32[1,2,64,16,64]{2,4,3,1,0:T(8,128)S(1)} %fusion.8, f32[2,64,16,64]{3,2,1,0:T(8,128)} %get-tuple-element.16, f32[1,16,64,64]{3,2,1,0:T(8,128)} %param.17, bf16[16,1,16,64,64]{4,3,2,1,0:T(8,128)(2,1)} %all-gather.11.cloned.1.call-done, ...), kind=kOutput, calls=%fused_computation.35 | convolution fusion | flops 107018240 | bytes 4829206 | tf_op jit(solution)/shard_map/snthd,shde->snthe/dot_general | solution.py:141
  602.2 3.7 fusion.5
  (163 shorter events, 92.9 us)
Async XLA Ops:
  7.2 137.0 %copy-start.1 = (bf16[1,128,2048]{2,1,0:T(8,128)(2,1)S(1)}, bf16[1,128,2048]{2,1,0:T(8,128)(2,1)}, u32[]{:S(2)}) copy-start(bf16[1,128,2048]{2,1,0:T(8,128)(2,1)} %param.10) | copy-start | bytes 1572868
  7.2 137.0 %copy-start.20 = (f32[1024]{0:T(1024)S(1)}, f32[1024]{0:T(1024)}, u32[]{:S(2)}) copy-start(f32[1024]{0:T(1024)} %param.15) | copy-start | bytes 12292
  7.2 137.0 %all-gather.9.cloned.1.call-start = ((), (), s32[]{:S(2)}) async-start(), calls=%async_computation.3 | async-start | bytes 4456448 | tf_op jit(solution)/shard_map/all_gather | solution.py:164
  8.0 181.2 %all-gather.7.cloned.1.call-start = ((), (), s32[]{:S(2)}) async-start(), calls=%async_computation.2 | async-start | bytes 4456448 | tf_op jit(solution)/shard_map/all_gather | solution.py:163
  8.8 254.8 %all-gather.5.cloned.1.call-start = ((), (), s32[]{:S(2)}) async-start(), calls=%async_computation.1 | async-start | bytes 4456448 | tf_op jit(solution)/shard_map/all_gather | solution.py:165
  9.6 373.5 %reduce-scatter.4.cloned.1.call-start = ((), (), s32[]{:S(2)}) async-start(), calls=%async_computation.5 | async-start | bytes 196608 | tf_op jit(solution)/shard_map/reduce_scatter | solution.py:74
  9.7 29.1 %collective-permute-start = (bf16[1024,128]{1,0:T(8,128)(2,1)}, bf16[1024,128]{1,0:T(8,128)(2,1)S(1)}, u32[]{:S(2)}, u32[]{:S(2)}) collective-permute-start(bf16[1024,128]{1,0:T(8,128)(2,1)} %param.19), channel_id=1, source_target_pairs={{0,8},{8,16},{16,24},{24,32},{32,40},{40,48},{48,56},{56,64},{64,7... | collective-permute-start | bytes 786440 | tf_op jit(solution)/shard_map/ppermute | solution.py:20
  38.8 110.1 %copy-start.3 = (bf16[1024,128]{1,0:T(8,128)(2,1)}, bf16[1024,128]{1,0:T(8,128)(2,1)S(1)}, u32[]{:S(2)}) copy-start(bf16[1024,128]{1,0:T(8,128)(2,1)S(1)} %collective-permute-done) | copy-start | bytes 786436
  38.8 15.1 %collective-permute-start.1 = (bf16[1024,128]{1,0:T(8,128)(2,1)S(1)}, bf16[1024,128]{1,0:T(8,128)(2,1)S(1)}, u32[]{:S(2)}, u32[]{:S(2)}) collective-permute-start(bf16[1024,128]{1,0:T(8,128)(2,1)S(1)} %collective-permute-done), channel_id=1, source_target_pairs={{0,8},{8,16},{16,24},{24,32},{32,40},{40,48},{48,56},{56,64},{64,7... | collective-permute-start | bytes 786440 | tf_op jit(solution)/shard_map/ppermute | solution.py:20
  38.8 15.2 %collective-permute-start.8 = (bf16[1024,128]{1,0:T(8,128)(2,1)}, bf16[1024,128]{1,0:T(8,128)(2,1)S(1)}, u32[]{:S(2)}, u32[]{:S(2)}) collective-permute-start(bf16[1024,128]{1,0:T(8,128)(2,1)} %param.19), channel_id=1, source_target_pairs={{0,120},{8,0},{16,8},{24,16},{32,24},{40,32},{48,40},{56,48},{64,5... | collective-permute-start | bytes 786440 | tf_op jit(solution)/shard_map/ppermute | solution.py:22
  53.9 94.9 %copy-start.5 = (bf16[1024,128]{1,0:T(8,128)(2,1)}, bf16[1024,128]{1,0:T(8,128)(2,1)S(1)}, u32[]{:S(2)}) copy-start(bf16[1024,128]{1,0:T(8,128)(2,1)S(1)} %collective-permute-done.1) | copy-start | bytes 786436
  53.9 15.0 %collective-permute-start.2 = (bf16[1024,128]{1,0:T(8,128)(2,1)S(1)}, bf16[1024,128]{1,0:T(8,128)(2,1)S(1)}, u32[]{:S(2)}, u32[]{:S(2)}) collective-permute-start(bf16[1024,128]{1,0:T(8,128)(2,1)S(1)} %collective-permute-done.1), channel_id=1, source_target_pairs={{0,8},{8,16},{16,24},{24,32},{32,40},{40,48},{48,56},{56,64},{64,7... | collective-permute-start | bytes 786440 | tf_op jit(solution)/shard_map/ppermute | solution.py:20
  53.9 94.9 %copy-start.4 = (bf16[1024,128]{1,0:T(8,128)(2,1)}, bf16[1024,128]{1,0:T(8,128)(2,1)S(1)}, u32[]{:S(2)}) copy-start(bf16[1024,128]{1,0:T(8,128)(2,1)S(1)} %collective-permute-done.8) | copy-start | bytes 786436
  53.9 15.0 %collective-permute-start.9 = (bf16[1024,128]{1,0:T(8,128)(2,1)S(1)}, bf16[1024,128]{1,0:T(8,128)(2,1)S(1)}, u32[]{:S(2)}, u32[]{:S(2)}) collective-permute-start(bf16[1024,128]{1,0:T(8,128)(2,1)S(1)} %collective-permute-done.8), channel_id=1, source_target_pairs={{0,120},{8,0},{16,8},{24,16},{32,24},{40,32},{48,40},{56,48},{64,5... | collective-permute-start | bytes 786440 | tf_op jit(solution)/shard_map/ppermute | solution.py:22
  68.9 79.9 %copy-start.7 = (bf16[1024,128]{1,0:T(8,128)(2,1)}, bf16[1024,128]{1,0:T(8,128)(2,1)S(1)}, u32[]{:S(2)}) copy-start(bf16[1024,128]{1,0:T(8,128)(2,1)S(1)} %collective-permute-done.2) | copy-start | bytes 786436
  68.9 14.6 %collective-permute-start.3 = (bf16[1024,128]{1,0:T(8,128)(2,1)S(1)}, bf16[1024,128]{1,0:T(8,128)(2,1)S(1)}, u32[]{:S(2)}, u32[]{:S(2)}) collective-permute-start(bf16[1024,128]{1,0:T(8,128)(2,1)S(1)} %collective-permute-done.2), channel_id=1, source_target_pairs={{0,8},{8,16},{16,24},{24,32},{32,40},{40,48},{48,56},{56,64},{64,7... | collective-permute-start | bytes 786440 | tf_op jit(solution)/shard_map/ppermute | solution.py:20
  68.9 79.9 %copy-start.6 = (bf16[1024,128]{1,0:T(8,128)(2,1)}, bf16[1024,128]{1,0:T(8,128)(2,1)S(1)}, u32[]{:S(2)}) copy-start(bf16[1024,128]{1,0:T(8,128)(2,1)S(1)} %collective-permute-done.9) | copy-start | bytes 786436
  68.9 14.6 %collective-permute-start.10 = (bf16[1024,128]{1,0:T(8,128)(2,1)S(1)}, bf16[1024,128]{1,0:T(8,128)(2,1)S(1)}, u32[]{:S(2)}, u32[]{:S(2)}) collective-permute-start(bf16[1024,128]{1,0:T(8,128)(2,1)S(1)} %collective-permute-done.9), channel_id=1, source_target_pairs={{0,120},{8,0},{16,8},{24,16},{32,24},{40,32},{48,40},{56,48},{64,5... | collective-permute-start | bytes 786440 | tf_op jit(solution)/shard_map/ppermute | solution.py:22
  83.5 65.4 %copy-start.10 = (bf16[1024,128]{1,0:T(8,128)(2,1)}, bf16[1024,128]{1,0:T(8,128)(2,1)S(1)}, u32[]{:S(2)}) copy-start(bf16[1024,128]{1,0:T(8,128)(2,1)S(1)} %collective-permute-done.3) | copy-start | bytes 786436
  83.5 14.7 %collective-permute-start.4 = (bf16[1024,128]{1,0:T(8,128)(2,1)S(1)}, bf16[1024,128]{1,0:T(8,128)(2,1)S(1)}, u32[]{:S(2)}, u32[]{:S(2)}) collective-permute-start(bf16[1024,128]{1,0:T(8,128)(2,1)S(1)} %collective-permute-done.3), channel_id=1, source_target_pairs={{0,8},{8,16},{16,24},{24,32},{32,40},{40,48},{48,56},{56,64},{64,7... | collective-permute-start | bytes 786440 | tf_op jit(solution)/shard_map/ppermute | solution.py:20
  83.5 65.4 %copy-start.8 = (bf16[1024,128]{1,0:T(8,128)(2,1)}, bf16[1024,128]{1,0:T(8,128)(2,1)S(1)}, u32[]{:S(2)}) copy-start(bf16[1024,128]{1,0:T(8,128)(2,1)S(1)} %collective-permute-done.10) | copy-start | bytes 786436
  83.5 16.0 %collective-permute-start.11 = (bf16[1024,128]{1,0:T(8,128)(2,1)S(1)}, bf16[1024,128]{1,0:T(8,128)(2,1)S(1)}, u32[]{:S(2)}, u32[]{:S(2)}) collective-permute-start(bf16[1024,128]{1,0:T(8,128)(2,1)S(1)} %collective-permute-done.10), channel_id=1, source_target_pairs={{0,120},{8,0},{16,8},{24,16},{32,24},{40,32},{48,40},{56,48},{64,5... | collective-permute-start | bytes 786440 | tf_op jit(solution)/shard_map/ppermute | solution.py:22
  98.1 14.3 %collective-permute-start.5 = (bf16[1024,128]{1,0:T(8,128)(2,1)S(1)}, bf16[1024,128]{1,0:T(8,128)(2,1)S(1)}, u32[]{:S(2)}, u32[]{:S(2)}) collective-permute-start(bf16[1024,128]{1,0:T(8,128)(2,1)S(1)} %collective-permute-done.4), channel_id=1, source_target_pairs={{0,8},{8,16},{16,24},{24,32},{32,40},{40,48},{48,56},{56,64},{64,7... | collective-permute-start | bytes 786440 | tf_op jit(solution)/shard_map/ppermute | solution.py:20
  99.5 14.4 %collective-permute-start.12 = (bf16[1024,128]{1,0:T(8,128)(2,1)S(1)}, bf16[1024,128]{1,0:T(8,128)(2,1)S(1)}, u32[]{:S(2)}, u32[]{:S(2)}) collective-permute-start(bf16[1024,128]{1,0:T(8,128)(2,1)S(1)} %collective-permute-done.11), channel_id=1, source_target_pairs={{0,120},{8,0},{16,8},{24,16},{32,24},{40,32},{48,40},{56,48},{64,5... | collective-permute-start | bytes 786440 | tf_op jit(solution)/shard_map/ppermute | solution.py:22
  112.4 8.8 %collective-permute-start.6 = (bf16[1024,128]{1,0:T(8,128)(2,1)S(1)}, bf16[1024,128]{1,0:T(8,128)(2,1)}, u32[]{:S(2)}, u32[]{:S(2)}) collective-permute-start(bf16[1024,128]{1,0:T(8,128)(2,1)S(1)} %collective-permute-done.5), channel_id=1, source_target_pairs={{0,8},{8,16},{16,24},{24,32},{32,40},{40,48},{48,56},{56,64},{64,7... | collective-permute-start | bytes 786440 | tf_op jit(solution)/shard_map/ppermute | solution.py:20
  113.9 14.2 %collective-permute-start.13 = (bf16[1024,128]{1,0:T(8,128)(2,1)S(1)}, bf16[1024,128]{1,0:T(8,128)(2,1)}, u32[]{:S(2)}, u32[]{:S(2)}) collective-permute-start(bf16[1024,128]{1,0:T(8,128)(2,1)S(1)} %collective-permute-done.12), channel_id=1, source_target_pairs={{0,120},{8,0},{16,8},{24,16},{32,24},{40,32},{48,40},{56,48},{64,5... | collective-permute-start | bytes 786440 | tf_op jit(solution)/shard_map/ppermute | solution.py:22
  121.2 10.2 %collective-permute-start.7 = (bf16[1024,128]{1,0:T(8,128)(2,1)}, bf16[1024,128]{1,0:T(8,128)(2,1)}, u32[]{:S(2)}, u32[]{:S(2)}) collective-permute-start(bf16[1024,128]{1,0:T(8,128)(2,1)} %collective-permute-done.6), channel_id=1, source_target_pairs={{0,8},{8,16},{16,24},{24,32},{32,40},{40,48},{48,56},{56,64},{64,7... | collective-permute-start | bytes 786440 | tf_op jit(solution)/shard_map/ppermute | solution.py:20
  128.1 261.2 %collective-permute-start.14 = (bf16[1024,128]{1,0:T(8,128)(2,1)}, bf16[1024,128]{1,0:T(8,128)(2,1)}, u32[]{:S(2)}, u32[]{:S(2)}) collective-permute-start(bf16[1024,128]{1,0:T(8,128)(2,1)} %collective-permute-done.13), channel_id=1, source_target_pairs={{0,120},{8,0},{16,8},{24,16},{32,24},{40,32},{48,40},{56,48},{64,5... | collective-permute-start | bytes 786440 | tf_op jit(solution)/shard_map/ppermute | solution.py:22
  365.4 54.7 %copy-start = (f32[2,64,16,64]{3,2,1,0:T(8,128)S(1)}, f32[2,64,16,64]{3,2,1,0:T(8,128)}, u32[]{:S(2)}) copy-start(f32[2,64,16,64]{3,2,1,0:T(8,128)} %get-tuple-element.13) | copy-start | bytes 1572868
  367.8 149.6 %all-reduce.6.cloned.1.call-start = ((), (), s32[]{:S(2)}) async-start(), calls=%async_computation.6 | async-start | bytes 131072
  383.1 208.1 %all-gather.11.cloned.1.call-start = ((), (), s32[]{:S(2)}) async-start(), calls=%async_computation.4 | async-start | bytes 4456448 | tf_op jit(solution)/shard_map/all_gather | solution.py:39
  418.7 172.6 %copy-start.19 = (f32[16,64]{1,0:T(8,128)S(1)}, f32[16,64]{1,0:T(8,128)}, u32[]{:S(2)}) copy-start(f32[16,64]{1,0:T(8,128)} %exp.349) | copy-start | bytes 12292
  (10 other events, 393.7 us)
Sparse Core Ops, SparseCore 0:
  9.8 103.6 all-gather.8
  115.3 73.8 all-gather.6
  191.0 72.4 all-gather.4
  367.9 13.5 reduce-scatter.3
  383.7 133.6 all-reduce.5
  519.1 72.1 all-gather.10
